TPU v7x, 32 devices: a whole 2x2x4 slice. The times are simulated.
32 devices in a mesh: sp: 4 (over z), tp: 8 (over y, x, core).
Axes of the slice: x: 2, y: 2, z: 4, core: 2. Of those that a mesh axis runs over, the one named last changes fastest.
Arguments:
- activations: bfloat16 [1024, 2048], P('sp', 'tp'), may hold values from -170 to 170
- norm_gain: float32 [2048], replicated, may hold values from 0.1 to 1.9
- query_weight: bfloat16 [2048, 1536], P(None, 'tp'), may hold values from -0.125 to 0.125
- latent_weight: bfloat16 [2048, 512], P(None, 'tp'), may hold values from -0.125 to 0.125
- rope_key_weight: bfloat16 [2048, 64], replicated, may hold values from -0.125 to 0.125
- latent_gain: float32 [512], replicated, may hold values from 1.5 to 64
- expand_weight: bfloat16 [512, 2048], P(None, 'tp'), may hold values from -0.25 to 0.25
- gate_weight: bfloat16 [2048, 1024], P(None, 'tp'), may hold values from -0.125 to 0.125
- pre_weight: bfloat16 [2048, 1024], P(None, 'tp'), may hold values from -0.125 to 0.125
- value_weight: bfloat16 [2048, 1024], P(None, 'tp'), may hold values from -0.125 to 0.125
- conv_kernel: bfloat16 [3, 1024], P(None, 'tp'), may hold values from -3.5 to 3.5
- output_attend: bfloat16 [1024, 2048], P('tp'), may hold values from -0.1875 to 0.1875
- output_conv: bfloat16 [1024, 2048], P('tp'), may hold values from -0.125 to 0.125
Outputs:
- mixed: bfloat16 [1024, 2048], P(('sp', 'tp'))
- log_weight_sum: float32 [8, 1024], P('tp', 'sp')
All inputs are finite; a program needn't handle non-finite values.
Results may differ from a plain program's by a relative error of at most 0.035.
The roundings to bfloat16 on the way count: a program that leaves them out, or rounds other values in their place, can miss the bound.
Values may be sent and summed in bfloat16 or wider, within the bound.
A program may use at most 128 MiB of HBM per device.

v0:
```python
import math

import jax
import jax.numpy as jnp
from jax import lax
from jax.sharding import PartitionSpec as P

D = 2048
NOPE = 128
ROPE = 64
VDIM = 128
GRID_W = 64


EPSILON = 1e-06
ROPE_BASE = 10000.0


def with_halo(array, sides, width):
    for axis, dim in sides:
        peers, length = (lax.axis_size(axis), array.shape[dim])
        up = [(i, (i + 1) % peers) for i in range(peers - 1)]
        down = [(j, i) for i, j in up]
        last = lax.slice_in_dim(array, length - width, length, axis=dim)
        leading = lax.slice_in_dim(array, 0, width, axis=dim)
        before = lax.ppermute(last, axis, up)
        after = lax.ppermute(leading, axis, down)
        array = jnp.concatenate([before, array, after], axis=dim)
    return array


def rotate(inputs, grid_rows, grid_cols):
    quarter = inputs.shape[-1] // 4
    inverse = ROPE_BASE ** (-jnp.arange(quarter, dtype=jnp.float32) / quarter)
    row_angle = (grid_rows[:, None] * inverse)[:, None, :]
    col_angle = (grid_cols[:, None] * inverse)[:, None, :]
    part_one = inputs[..., :quarter]
    part_two = inputs[..., quarter : 2 * quarter]
    part_three = inputs[..., 2 * quarter : 3 * quarter]
    part_four = inputs[..., 3 * quarter :]
    return jnp.concatenate(
        [
            part_one * jnp.cos(row_angle) - part_two * jnp.sin(row_angle),
            part_one * jnp.sin(row_angle) + part_two * jnp.cos(row_angle),
            part_three * jnp.cos(col_angle) - part_four * jnp.sin(col_angle),
            part_three * jnp.sin(col_angle) + part_four * jnp.cos(col_angle),
        ],
        axis=-1,
    )


def conv_branch(gate_proj, pre_proj, value_proj, conv_kernel):
    pre_mix = (pre_proj * value_proj).astype(jnp.bfloat16)
    padded = with_halo(pre_mix, (("sp", 0),), 1).astype(jnp.float32)
    kernel = conv_kernel.astype(jnp.float32)
    convolved = kernel[0] * padded[:-2] + kernel[1] * padded[1:-1] + kernel[2] * padded[2:]
    return (gate_proj * convolved).astype(jnp.bfloat16)


def body(
    activations,
    norm_gain,
    query_weight,
    latent_weight,
    rope_key_weight,
    latent_gain,
    expand_weight,
    gate_weight,
    pre_weight,
    value_weight,
    conv_kernel,
    output_attend,
    output_conv,
):
    tokens_here = activations.shape[0]
    query_cols = query_weight.shape[1]
    heads_here = query_cols // (NOPE + ROPE)
    latent_cols = latent_weight.shape[1]
    channels = gate_weight.shape[1]
    joined = jnp.concatenate(
        [query_weight, latent_weight, rope_key_weight, gate_weight, pre_weight, value_weight],
        axis=1,
    )
    inputs_f32 = activations.astype(jnp.float32)
    squares = lax.psum(jnp.sum(inputs_f32 * inputs_f32, axis=1, keepdims=True), "tp")
    partial_squares = jnp.zeros((tokens_here, 1), jnp.float32)
    piece_f32 = lax.all_gather(activations, "tp", axis=1, tiled=True).astype(jnp.float32)
    scaled = (piece_f32 * norm_gain).astype(jnp.bfloat16)
    running = jnp.dot(scaled, joined, preferred_element_type=jnp.float32)
    running, folded_squares = (running, partial_squares)
    inv_rms = lax.rsqrt(squares / D + EPSILON)
    projected = running * inv_rms
    latent_end = query_cols + latent_cols
    rope_end = latent_end + ROPE
    query_proj = projected[:, :query_cols]
    latent_proj = projected[:, query_cols:latent_end]
    rope_proj = projected[:, latent_end:rope_end]
    gate_proj = projected[:, rope_end : rope_end + channels]
    pre_proj = projected[:, rope_end + channels : rope_end + 2 * channels]
    value_proj = projected[:, rope_end + 2 * channels :]
    positions = lax.axis_index("sp") * tokens_here + jnp.arange(tokens_here, dtype=jnp.int32)
    grid_rows = (positions // GRID_W).astype(jnp.float32)
    grid_cols = (positions % GRID_W).astype(jnp.float32)
    query = query_proj.reshape(tokens_here, heads_here, NOPE + ROPE)
    query = jnp.concatenate(
        [query[..., :NOPE], rotate(query[..., NOPE:], grid_rows, grid_cols)], axis=-1
    )
    query = (query * (NOPE + ROPE) ** (-0.5)).astype(jnp.bfloat16)
    query_nope = query[..., :NOPE]
    query_rope = query[..., NOPE:]
    gathered = lax.all_gather(latent_proj.astype(jnp.bfloat16), "tp", axis=1, tiled=True).astype(
        jnp.float32
    )
    latent = (
        gathered
        * lax.rsqrt(jnp.mean(gathered * gathered, axis=1, keepdims=True) + EPSILON)
        * latent_gain
    ).astype(jnp.bfloat16)
    expanded = jnp.dot(latent, expand_weight, preferred_element_type=jnp.float32).astype(
        jnp.bfloat16
    )
    rope_key = rotate(rope_proj[:, None, :], grid_rows, grid_cols)[:, 0].astype(jnp.bfloat16)
    starting = (
        jnp.full((heads_here, tokens_here), -jnp.inf, jnp.float32),
        jnp.zeros((heads_here, tokens_here), jnp.float32),
        jnp.zeros((tokens_here, heads_here, VDIM), jnp.float32),
    )
    key_piece = lax.all_gather(expanded, "sp", axis=0, tiled=True)
    rope_piece = lax.all_gather(rope_key, "sp", axis=0, tiled=True)
    piece_rows = key_piece.shape[0]
    key_block = math.gcd(piece_rows, 1024)
    split_heads = key_piece.reshape(piece_rows, heads_here, NOPE + VDIM)

    def one_block(turn_index, state):
        row_max, row_sum, running_out = state
        offset = turn_index * key_block
        block_keys = lax.dynamic_slice_in_dim(split_heads, offset, key_block, 0)
        block_rope = lax.dynamic_slice_in_dim(rope_piece, offset, key_block, 0)
        scores = jnp.einsum(
            "thd,jhd->htj", query_nope, block_keys[..., :NOPE], preferred_element_type=jnp.float32
        )
        scores = scores + jnp.einsum(
            "thd,jd->htj", query_rope, block_rope, preferred_element_type=jnp.float32
        )
        new_max = jnp.maximum(row_max, jnp.max(scores, axis=-1))
        rescale = jnp.exp(row_max - new_max)
        weights = jnp.exp(scores - new_max[..., None])
        row_sum = row_sum * rescale + jnp.sum(weights, axis=-1)
        running_out = running_out * rescale.T[..., None] + jnp.einsum(
            "htj,jhd->thd",
            weights.astype(jnp.bfloat16),
            block_keys[..., NOPE:],
            preferred_element_type=jnp.float32,
        )
        return (new_max, row_sum, running_out)

    row_max, row_sum, running_out = lax.fori_loop(0, piece_rows // key_block, one_block, starting)
    attended = (
        (running_out / row_sum.T[..., None])
        .astype(jnp.bfloat16)
        .reshape(tokens_here, heads_here * VDIM)
    )
    log_weight_sum = row_max + jnp.log(row_sum)
    conv_mixed = conv_branch(gate_proj, pre_proj, value_proj, conv_kernel)
    mixed = lax.psum_scatter(
        (
            jnp.dot(attended, output_attend, preferred_element_type=jnp.float32)
            + jnp.dot(conv_mixed, output_conv, preferred_element_type=jnp.float32)
        ).astype(jnp.bfloat16),
        "tp",
        scatter_dimension=0,
        tiled=True,
    )
    return (mixed, log_weight_sum)


def solution(mesh):
    return jax.shard_map(
        body,
        mesh=mesh,
        in_specs=(
            P("sp", "tp"),
            P(),
            P(None, "tp"),
            P(None, "tp"),
            P(),
            P(),
            P(None, "tp"),
            P(None, "tp"),
            P(None, "tp"),
            P(None, "tp"),
            P(None, "tp"),
            P("tp", None),
            P("tp", None),
        ),
        out_specs=(P(("sp", "tp"), None), P("tp", "sp")),
        check_vma=False,
    )
```

profile of v0, /device:TPU:0, one launch (start us, length us, event | category | flops | bytes accessed | tf_op | source)
XLA Modules:
  0.0 135.6 jit_solution(17453811287171782455)
XLA Ops:
  7.2 0.0 copy-start
  7.2 0.0 copy-start.5
  7.2 0.0 copy-start.1
  7.2 0.0 copy-start.3
  7.2 0.0 copy-start.4
  7.2 0.0 all-gather.3.cloned.1.call-start
  7.3 0.7 all-gather.3.cloned.1.call-update
  8.0 0.0 reduce-scatter.2.cloned.1.call-start
  8.0 1.0 multiply_reduce_fusion
  9.0 1.2 copy.19
  10.3 1.3 copy.20
  11.5 1.2 copy.21
  12.8 15.2 %psum.7 = f32[256,1]{0,1:T(1,128)S(1)} all-reduce(f32[256,1]{0,1:T(1,128)S(1)} %bitcast.73), channel_id=1, replica_groups=mesh['sp'=4,'tp'=8] {'tp'}, use_global_device_ids=true, to_apply=%region_1.0 | all-reduce | flops 256 | bytes 2048 | tf_op jit(solution)/shard_map/psum | solution.py:85
  28.0 0.0 copy-done.5
  28.0 0.6 slice_bitcast_fusion.13
  28.6 0.0 copy-done.1
  28.6 0.0 copy-start.7
  28.6 0.9 constant_dynamic-update-slice_fusion.5
  29.5 0.0 copy-done.3
  29.6 0.7 constant_dynamic-update-slice_fusion.4
  30.3 0.0 copy-done.4
  30.3 0.7 constant_dynamic-update-slice_fusion.3
  31.0 0.8 constant_dynamic-update-slice_fusion.2
  31.8 0.9 constant_dynamic-update-slice_fusion.1
  32.7 0.8 constant_dynamic-update-slice_fusion
  33.5 2.7 %all-gather.3.cloned.1.call-done = bf16[256,2048]{1,0:T(8,128)(2,1)} async-done(((bf16[256,256]{1,0:T(8,128)(2,1)}), bf16[256,2048]{1,0:T(8,128)(2,1)}) %all-gather.3.cloned.1.call-update) | async-done | bytes 1048592 | tf_op jit(solution)/shard_map/all_gather | solution.py:87
  36.2 0.0 copy-done.7
  36.2 0.0 copy-start.6
  36.2 0.0 copy-start.8
  36.2 3.1 %convolution_multiply_fusion = f32[256,704]{0,1:T(8,128)S(1)} fusion(bf16[2048,704]{0,1:T(8,128)(2,1)} %constant_dynamic-update-slice_fusion, bf16[256,2048]{1,0:T(8,128)(2,1)} %all-gather.3.cloned.1.call-done, f32[2048]{0:T(1024)S(1)} %copy-done.7, f32[256]{0:T(256)S(1)} %bitcast.74), kind=kOutput, calls=%fused_computation.6 | convolution fusion | flops 739950592 | bytes 4662272 | tf_op jit(solution)/shard_map/dot_general | solution.py:89
  39.4 0.1 constant_dynamic-update-slice_fusion.9
  39.6 0.1 constant_dynamic-update-slice_fusion.8
  39.7 0.2 fusion.52
  39.9 13.4 %all-gather = bf16[1024,1,64]{0,2,1:T(8,128)(2,1)S(1)} all-gather(bf16[256,1,64]{0,2,1:T(8,128)(2,1)S(1)} %pad_maximum_fusion), channel_id=2, replica_groups=mesh['sp'=4,'tp'=8] {'sp'}, dimensions={0}, use_global_device_ids=true | all-gather | bytes 163840 | tf_op jit(solution)/shard_map/all_gather | solution.py:129
  53.4 0.1 constant_dynamic-update-slice_fusion.6
  53.5 9.3 %all_gather.13 = bf16[256,512]{0,1:T(8,128)(2,1)S(1)} all-gather(bf16[256,64]{0,1:T(8,128)(2,1)S(1)} %slice.196), channel_id=1, replica_groups=mesh['sp'=4,'tp'=8] {'tp'}, dimensions={1}, use_global_device_ids=true | all-gather | bytes 294912 | tf_op jit(solution)/shard_map/all_gather | solution.py:111
  62.8 0.1 fusion.10
  62.9 0.0 copy-done.6
  62.9 0.0 copy-done.8
  62.9 0.4 convolution_convert_fusion
  63.3 16.1 %all_gather.14 = bf16[1024,256]{1,0:T(8,128)(2,1)S(1)} all-gather(bf16[256,256]{1,0:T(8,128)(2,1)S(1)} %convolution_convert_fusion), channel_id=1, replica_groups=mesh['sp'=4,'tp'=8] {'sp'}, dimensions={0}, use_global_device_ids=true | all-gather | bytes 655360 | tf_op jit(solution)/shard_map/all_gather | solution.py:128
  79.4 0.3 convolution_bitcast_fusion.1
  79.7 0.4 fusion.66
  80.1 0.0 copy-start.2
  80.2 0.3 fusion.7
  80.5 0.1 fusion.65
  80.5 3.7 %collective-permute-start = (bf16[1,128]{0,1:T(8,128)(2,1)S(1)}, bf16[1,128]{0,1:T(8,128)(2,1)S(1)}, u32[]{:S(2)}, u32[]{:S(2)}) collective-permute-start(bf16[1,128]{0,1:T(8,128)(2,1)S(1)} %get-tuple-element.26), channel_id=1, source_target_pairs={{0,8},{8,16},{16,24},{1,9},{9,17},{17,25},{2,10},{10,18},{18,26},{... | collective-permute-start | bytes 776 | tf_op jit(solution)/shard_map/ppermute | solution.py:26
  84.2 1.3 collective-permute-start.1
  85.5 0.0 copy-done
  85.5 2.4 %fusion.9 = f32[256,2048]{1,0:T(8,128)} fusion(bf16[128,2048]{1,0:T(8,128)(2,1)S(1)} %copy-done, f32[1,256,1024]{2,1,0:T(8,128)S(1)} %get-tuple-element.44, f32[256]{0:T(256)S(1)} %get-tuple-element.43, bf16[1024,1,256]{2,0,1:T(8,128)(2,1)S(1)} %bitcast.70, f32[256]{0:T(256)S(1)} %get-tuple-element.42, f32[256]{0:T(256)S(1)} %get-tuple-element.41), kind=kOutput, calls=%fused_computation.19 | convolution fusion | flops 201949184 | bytes 3935232 | tf_op jit(solution)/shard_map/dot_general | solution.py:167
  88.0 0.0 collective-permute-done
  88.0 2.1 %collective-permute-done.1 = bf16[1,128]{0,1:T(8,128)(2,1)S(1)} collective-permute-done((bf16[1,128]{0,1:T(8,128)(2,1)S(1)}, bf16[1,128]{0,1:T(8,128)(2,1)S(1)}, u32[]{:S(2)}, u32[]{:S(2)}) %collective-permute-start.1) | collective-permute-done | bytes 288 | tf_op jit(solution)/shard_map/ppermute | solution.py:27
  90.0 0.1 maximum_convert_fusion
  90.2 0.0 copy-done.2
  90.2 3.2 %fusion = bf16[256,2048]{1,0:T(8,128)(2,1)} fusion(f32[256,2048]{1,0:T(8,128)} %fusion.9, bf16[128,2048]{1,0:T(8,128)(2,1)S(1)} %copy-done.2, f32[258,128]{0,1:T(8,128)S(1)} %maximum_convert_fusion, f32[256,704]{0,1:T(8,128)S(1)} %convolution_multiply_fusion, f32[128]{0:T(128)} %get-tuple-element.38, f32[128]{0:T(128)} %get-tuple-element.39, ...), kind=kOutput, calls=%fused_computation.1 | convolution fusion | flops 135495680 | bytes 4195840 | tf_op jit(solution)/shard_map/dot_general | solution.py:168
  93.4 0.0 reduce-scatter.2.cloned.1.call-update
  93.4 0.6 log_add_fusion
  94.0 34.8 %reduce-scatter.2.cloned.1.call-done = bf16[32,2048]{1,0:T(8,128)(2,1)} async-done(((bf16[256,2048]{1,0:T(8,128)(2,1)}), bf16[32,2048]{1,0:T(8,128)(2,1)}) %reduce-scatter.2.cloned.1.call-update) | async-done | bytes 131088 | tf_op jit(solution)/shard_map/reduce_scatter | solution.py:165
  (13 shorter events, 0.1 us)
Async XLA Ops:
  7.2 78.4 %copy-start = (bf16[128,2048]{1,0:T(8,128)(2,1)S(1)}, bf16[128,2048]{1,0:T(8,128)(2,1)}, u32[]{:S(2)}) copy-start(bf16[128,2048]{1,0:T(8,128)(2,1)} %param.24) | copy-start | bytes 1572868
  7.2 20.8 %copy-start.5 = (bf16[3,128]{1,0:T(4,128)(2,1)S(1)}, bf16[3,128]{1,0:T(4,128)(2,1)}, u32[]{:S(2)}) copy-start(bf16[3,128]{1,0:T(4,128)(2,1)} %param.23) | copy-start | bytes 2308
  7.2 21.4 %copy-start.1 = (bf16[2048,192]{0,1:T(8,128)(2,1)S(1)}, bf16[2048,192]{0,1:T(8,128)(2,1)}, u32[]{:S(2)}) copy-start(bf16[2048,192]{0,1:T(8,128)(2,1)} %param.15) | copy-start | bytes 2359300
  7.2 22.3 %copy-start.3 = (bf16[2048,64]{0,1:T(8,128)(2,1)S(1)}, bf16[2048,64]{0,1:T(8,128)(2,1)}, u32[]{:S(2)}) copy-start(bf16[2048,64]{0,1:T(8,128)(2,1)} %param.16) | copy-start | bytes 786436
  7.2 23.1 %copy-start.4 = (bf16[2048,64]{0,1:T(8,128)(2,1)S(1)}, bf16[2048,64]{0,1:T(8,128)(2,1)}, u32[]{:S(2)}) copy-start(bf16[2048,64]{0,1:T(8,128)(2,1)} %param.17) | copy-start | bytes 786436
  7.2 29.0 %all-gather.3.cloned.1.call-start = ((), (), s32[]{:S(2)}) async-start(), calls=%async_computation.1 | async-start | bytes 1179648 | tf_op jit(solution)/shard_map/all_gather | solution.py:87
  8.0 120.8 %reduce-scatter.2.cloned.1.call-start = ((), (), s32[]{:S(2)}) async-start(), calls=%async_computation.2 | async-start | bytes 1179648 | tf_op jit(solution)/shard_map/reduce_scatter | solution.py:165
  28.6 7.6 %copy-start.7 = (f32[2048]{0:T(1024)S(1)}, f32[2048]{0:T(1024)}, u32[]{:S(2)}) copy-start(f32[2048]{0:T(1024)} %param.14) | copy-start | bytes 24580
  36.2 26.7 %copy-start.6 = (bf16[512,256]{1,0:T(8,128)(2,1)S(1)}, bf16[512,256]{1,0:T(8,128)(2,1)}, u32[]{:S(2)}) copy-start(bf16[512,256]{1,0:T(8,128)(2,1)} %param.19) | copy-start | bytes 786436
  36.2 26.7 %copy-start.8 = (f32[512]{0:T(512)S(1)}, f32[512]{0:T(512)}, u32[]{:S(2)}) copy-start(f32[512]{0:T(512)} %param.18) | copy-start | bytes 6148
  80.1 10.0 %copy-start.2 = (bf16[128,2048]{1,0:T(8,128)(2,1)S(1)}, bf16[128,2048]{1,0:T(8,128)(2,1)}, u32[]{:S(2)}) copy-start(bf16[128,2048]{1,0:T(8,128)(2,1)} %param.25) | copy-start | bytes 1572868
  80.5 7.4 %collective-permute-start = (bf16[1,128]{0,1:T(8,128)(2,1)S(1)}, bf16[1,128]{0,1:T(8,128)(2,1)S(1)}, u32[]{:S(2)}, u32[]{:S(2)}) collective-permute-start(bf16[1,128]{0,1:T(8,128)(2,1)S(1)} %get-tuple-element.26), channel_id=1, source_target_pairs={{0,8},{8,16},{16,24},{1,9},{9,17},{17,25},{2,10},{10,18},{18,26},{... | collective-permute-start | bytes 776 | tf_op jit(solution)/shard_map/ppermute | solution.py:26
  84.2 5.8 %collective-permute-start.1 = (bf16[1,128]{0,1:T(8,128)(2,1)S(1)}, bf16[1,128]{0,1:T(8,128)(2,1)S(1)}, u32[]{:S(2)}, u32[]{:S(2)}) collective-permute-start(bf16[1,128]{0,1:T(8,128)(2,1)S(1)} %get-tuple-element.36), channel_id=1, source_target_pairs={{8,0},{16,8},{24,16},{9,1},{17,9},{25,17},{10,2},{18,10},{26,18},{... | collective-permute-start | bytes 776 | tf_op jit(solution)/shard_map/ppermute | solution.py:27
Sparse Core Ops, SparseCore 0:
  9.9 26.2 all-gather.2
  93.5 35.1 reduce-scatter.1
where the time goes:
time: 136 us
  blocking collectives  53.9 us (40%)
  waiting for transfers between devices  40.2 us (30%)
  between operations  14.3 us (11%)
  matrix products  9.9 us (7%)
  local copies, waits for them, and re-layouts  9.39 us (7%)
  starting transfers between devices  5.04 us (4%)
  other arithmetic  2.83 us (2%)
    reduce_scatter x1, waiting for transfers between devices, body(): lax.psum_scatter((jnp.dot(attended, output_attend, preferred_element_type...  34.8 us
    all_gather x1, blocking collectives, body(): key_piece = lax.all_gather(expanded, 'sp', axis=0, tiled=True)  16.1 us
    psum x1, blocking collectives, body(): lax.psum(jnp.sum(inputs_f32 * inputs_f32, axis=1, keepdims=True), 'tp')  15.2 us
    all_gather x1, blocking collectives, body(): rope_piece = lax.all_gather(rope_key, 'sp', axis=0, tiled=True)  13.4 us
    all_gather x1, blocking collectives, body(): lax.all_gather(latent_proj.astype(jnp.bfloat16), 'tp', axis=1, tiled=True)  9.26 us
    unnamed x27, local copies, waits for them, and re-layouts  7.86 us
    ppermute x1, starting transfers between devices, with_halo(): before = lax.ppermute(last, axis, up)  3.67 us
    dot_general x1, matrix products, body(): jnp.dot(conv_mixed, output_conv, preferred_element_type=jnp.float32)  3.22 us
  transfers between devices with their start and end apart: 4, of which 3 were waited for; matrix products, arithmetic and copies ran while one was open for 10% of the time, Pallas kernels for 0%

commit v1 on v0

--- a/solution.py
+++ b/solution.py
@@ -1,8 +1,12 @@
+import functools
 import math
 
 import jax
 import jax.numpy as jnp
+import numpy as np
 from jax import lax
+from jax.experimental import pallas as pl
+from jax.experimental.pallas import tpu as pltpu
 from jax.sharding import PartitionSpec as P
 
 D = 2048
@@ -174,9 +178,490 @@
     return (mixed, log_weight_sum)
 
 
+CORES = 2
+MAX_SPLITS = 8
+OUT_CHUNKS = 4
+MESH = pl.DeviceIdType.MESH
+
+
+def fits(mesh):
+    chips = mesh.shape["tp"] // CORES
+    return mesh.shape["sp"] <= MAX_SPLITS and chips & (chips - 1) == 0
+
+
+def flip(index, mask, count):
+    total, bit = 0, 1
+    while bit < count:
+        has = (index // bit) % 2
+        total = total + bit * ((1 - has) if mask & bit else has)
+        bit *= 2
+    return total
+
+
+def rope_table(tokens):
+    quarter = ROPE // 4
+    inverse = np.float32(ROPE_BASE) ** (-np.arange(quarter, dtype=np.float32) / np.float32(quarter))
+    place = np.arange(tokens)
+    row = (place // GRID_W).astype(np.float32)[:, None] * inverse.astype(np.float32)
+    col = (place % GRID_W).astype(np.float32)[:, None] * inverse.astype(np.float32)
+    parts = [np.cos(row), np.cos(row), np.cos(col), np.cos(col)]
+    parts += [-np.sin(row), np.sin(row), -np.sin(col), np.sin(col)]
+    return np.concatenate(parts, axis=1).astype(np.float32)
+
+
+def turn(z, cos, sin):
+    lane = lax.broadcasted_iota(jnp.int32, z.shape, 1)
+    quarter = ROPE // 4
+    other = jnp.where(lane % (2 * quarter) < quarter, pltpu.roll(z, 128 - quarter, 1), pltpu.roll(z, quarter, 1))
+    return z * cos + other * sin
+
+
+def mixer_kernel(
+    splits,
+    chips,
+    act,
+    gain,
+    wq_h,
+    wl_h,
+    wr_h,
+    lat_gain,
+    we_h,
+    wg_h,
+    wp_h,
+    wv_h,
+    taps,
+    oa_h,
+    oc_h,
+    tab_h,
+    out_ref,
+    lse_ref,
+    actb,
+    wq,
+    wl,
+    wr,
+    we,
+    wg,
+    wp,
+    wv,
+    wo,
+    tab,
+    acc_l,
+    acc_g,
+    acc_q,
+    latb,
+    ropeb,
+    halo_out,
+    halo_in,
+    qcat,
+    kcat,
+    vals,
+    scores,
+    pads,
+    pbuf,
+    pair_in,
+    pair_sum,
+    chip_in,
+    in_sem,
+    act_send,
+    act_recv,
+    lat_send,
+    lat_recv,
+    rope_send,
+    rope_recv,
+    halo_send,
+    halo_recv,
+    pair_send,
+    pair_recv,
+    chip_send,
+    chip_recv,
+):
+    f32, bf16 = jnp.float32, jnp.bfloat16
+    sp, tp = lax.axis_index("sp"), lax.axis_index("tp")
+    core, chip = tp % CORES, tp // CORES
+    tokens, local = act.shape
+    half = tokens // 2
+    partner = (sp, chip * CORES + 1 - core)
+    chip_of = [flip(chip, m, chips) for m in range(chips)]
+    mate = [(sp, chip_of[m] * CORES + core) for m in range(chips)]
+    far = [((sp + d) % splits, tp) for d in range(splits)]
+    near_first = list(range(1, chips))
+    far_first = near_first[::-1]
+
+    def remote(source, target, send, recv, device):
+        return pltpu.make_async_remote_copy(
+            src_ref=source, dst_ref=target, send_sem=send, recv_sem=recv,
+            device_id=device, device_id_type=MESH,
+        )
+
+    loads = [
+        (act, actb.at[0, core]), (wl_h, wl), (wr_h, wr), (wq_h, wq), (wg_h, wg), (wp_h, wp), (wv_h, wv),
+        (tab_h.at[pl.ds(sp * tokens, tokens)], tab), (we_h, we),
+        (oa_h, wo.at[pl.ds(0, oa_h.shape[0])]), (oc_h, wo.at[pl.ds(oa_h.shape[0], oc_h.shape[0])]),
+    ]
+    loads = [pltpu.make_async_copy(a, b, in_sem.at[i]) for i, (a, b) in enumerate(loads)]
+    for load in loads:
+        load.start()
+
+    barrier = pltpu.get_barrier_semaphore()
+    peers = [partner] + mate[1:] + far[1:]
+    for peer in peers:
+        pl.semaphore_signal(barrier, inc=1, device_id=peer, device_id_type=MESH)
+    pl.semaphore_wait(barrier, len(peers))
+
+    pending = []
+    loads[0].wait()
+    own = actb.at[0, core]
+
+    def send_act(m):
+        copy = remote(own, actb.at[m, core], act_send.at[m], act_recv.at[m, 0], mate[m])
+        copy.start()
+        pending.append(copy)
+        return copy
+
+    def pass_act(m):
+        copy = remote(actb.at[m, core], actb.at[m, core], act_send.at[chips + m], act_recv.at[m, 1], partner)
+        copy.start()
+        pending.append(copy)
+        return copy
+
+    direct = {m: send_act(m) for m in far_first}
+    passed = {0: pass_act(0)}
+    for load in loads[1:8]:
+        load.wait()
+
+    squares = jnp.zeros((tokens, 128), f32)
+    scaled = {}
+
+    def rows_of(m, k):
+        return pl.ds(pl.multiple_of((chip_of[m] * CORES + k) * local, local), local)
+
+    def scale(m, squares):
+        for k in range(CORES):
+            x = actb[m, k].astype(f32)
+            for c in range(0, local, 128):
+                squares = squares + x[:, c : c + 128] * x[:, c : c + 128]
+            scaled[m, k] = (x * gain[:, rows_of(m, k)]).astype(bf16)
+        return squares
+
+    def put(ref, value, first):
+        if first:
+            ref[...] = value
+        else:
+            ref[...] += value
+
+    def latent_dot(m):
+        for k in range(CORES):
+            rows = rows_of(m, k)
+            weight = jnp.concatenate([wl[rows, :], wr[rows, :]], axis=1)
+            put(acc_l, jnp.dot(scaled[m, k], weight, preferred_element_type=f32), m == 0 and k == 0)
+
+    def other_dots(m):
+        for k in range(CORES):
+            rows = rows_of(m, k)
+            first = m == 0 and k == 0
+            weight = jnp.concatenate([wg[rows, :], wp[rows, :], wv[rows, :]], axis=1)
+            put(acc_g, jnp.dot(scaled[m, k], weight, preferred_element_type=f32), first)
+            put(acc_q, jnp.dot(scaled[m, k], wq[rows, :], preferred_element_type=f32), first)
+
+    passed[0].wait_recv()
+    squares = scale(0, squares)
+    latent_dot(0)
+    other_dots(0)
+    for m in near_first:
+        direct[m].wait_recv()
+        passed[m] = pass_act(m)
+        if m > 1:
+            passed[m - 1].wait_recv()
+            squares = scale(m - 1, squares)
+            latent_dot(m - 1)
+            other_dots(m - 1)
+    last = chips - 1
+    passed[last].wait_recv()
+    squares = scale(last, squares)
+    latent_dot(last)
+    inv_rms = lax.rsqrt(jnp.sum(squares, axis=1, keepdims=True) / (local * chips * CORES) + EPSILON)
+
+    lane = lax.broadcasted_iota(jnp.int32, (half, 128), 1)
+    proj = acc_l[...] * inv_rms
+    low, high = proj[:half], proj[half:]
+    latb[0, 0, core] = jnp.where(lane < 64, low, pltpu.roll(high, 64, 1)).astype(bf16)
+
+    def send_lat(d, m, index, recv, device, slot):
+        copy = remote(latb.at[d, m, core], latb.at[slot[0], slot[1], core], lat_send.at[index], recv, device)
+        copy.start()
+        pending.append(copy)
+        return copy
+
+    count = 0
+    lat_direct, lat_pass, lat_far = {}, {}, {}
+    for d in [d for d in (2, 1, 3) if d < splits] + list(range(4, splits)):
+        lat_far[d] = send_lat(0, 0, count, lat_recv.at[(splits - d) % splits, 0, 0], far[d], ((splits - d) % splits, 0))
+        count += 1
+
+    def spread(d, count):
+        for m in far_first:
+            lat_direct[d, m] = send_lat(d, 0, count, lat_recv.at[d, m, 0], mate[m], (d, m))
+            count += 1
+        lat_pass[d, 0] = send_lat(d, 0, count, lat_recv.at[d, 0, 1], partner, (d, 0))
+        return count + 1
+
+    count = spread(0, count)
+
+    table = tab[...]
+    wide = lax.broadcasted_iota(jnp.int32, (tokens, 128), 1)
+    shifted = pltpu.roll(table, 64, 1)
+    cos = jnp.where(wide < 64, table, shifted)
+    sin = jnp.where(wide < 64, shifted, table)
+    raw = jnp.where(lane < 64, pltpu.roll(low, 64, 1), high)
+    ropeb[0] = turn(
+        raw,
+        jnp.where(lane < 64, cos[:half], cos[half:]),
+        jnp.where(lane < 64, sin[:half], sin[half:]),
+    ).astype(bf16)
+    rope_far = {}
+    for d in range(1, splits):
+        back = (splits - d) % splits
+        rope_far[back] = remote(ropeb.at[0], ropeb.at[back], rope_send.at[d], rope_recv.at[back], far[d])
+        rope_far[back].start()
+        pending.append(rope_far[back])
+
+    other_dots(last)
+
+    def far_wait(d):
+        lat_far[(splits - d) % splits].wait_recv()
+
+    premix = (acc_g[:, 128:256] * inv_rms) * (acc_g[:, 256:] * inv_rms)
+    premix = premix.astype(bf16)
+    rim = halo_out.shape[1]
+    halo_out[0] = premix[tokens - rim :]
+    halo_out[1] = premix[:rim]
+    halos = [
+        remote(halo_out.at[0], halo_in.at[0], halo_send.at[0], halo_recv.at[0], far[1]),
+        remote(halo_out.at[1], halo_in.at[1], halo_send.at[1], halo_recv.at[1], far[splits - 1]),
+    ]
+    for copy in halos:
+        copy.start()
+        pending.append(copy)
+
+    order = [0] + [d for d in (1, 3, 2) if d < splits] + list(range(4, splits))
+    for d in order[1:]:
+        far_wait(d)
+        count = spread(d, count)
+
+    factor = (NOPE + ROPE) ** (-0.5)
+    qcat[:, :NOPE] = (acc_q[:, :NOPE] * inv_rms * factor).astype(bf16)
+    tail = jnp.concatenate([acc_q[:, NOPE:], jnp.zeros((tokens, 128 - ROPE), f32)], axis=1) * inv_rms
+    qcat[:, NOPE:] = jnp.where(wide < 64, turn(tail, cos, sin) * factor, 0.0).astype(bf16)
+
+    for load in loads[8:]:
+        load.wait()
+
+    def pass_lat(d, count):
+        for m in near_first:
+            lat_direct[d, m].wait_recv()
+            lat_pass[d, m] = send_lat(d, m, count, lat_recv.at[d, m, 1], partner, (d, m))
+            count += 1
+        return count
+
+    def conv():
+        pads[8 : 8 + tokens] = premix.astype(f32)
+        for copy in halos:
+            copy.wait_recv()
+        before = jnp.where(sp > 0, halo_in[0].astype(f32)[rim - 1 :], 0.0)
+        after = jnp.where(sp < splits - 1, halo_in[1].astype(f32)[:1], 0.0)
+        pads[7:8] = before
+        pads[8 + tokens : 9 + tokens] = after
+        tap = taps[...].astype(f32)
+        mixed = tap[0:1] * pads[7 : 7 + tokens] + tap[1:2] * pads[8 : 8 + tokens] + tap[2:3] * pads[9 : 9 + tokens]
+        return ((acc_g[:, :128] * inv_rms) * mixed).astype(bf16)
+
+    def expand(d):
+        low, high = [], []
+        weight = []
+        for m in range(chips):
+            a, b = latb[d, m, 0].astype(f32), latb[d, m, 1].astype(f32)
+            low.append(jnp.where(lane < 64, a, pltpu.roll(b, 64, 1)))
+            high.append(jnp.where(lane < 64, pltpu.roll(a, 64, 1), b))
+            weight.append(we[pl.ds(pl.multiple_of(chip_of[m] * 128, 128), 128), :])
+        weight = jnp.concatenate(weight, axis=0)
+        for side, parts in enumerate((low, high)):
+            total = sum(p * p for p in parts)
+            root = lax.rsqrt(jnp.sum(total, axis=1, keepdims=True) / (128 * chips) + EPSILON)
+            parts = [
+                (p * root * lat_gain[:, pl.ds(pl.multiple_of(chip_of[m] * 128, 128), 128)]).astype(bf16)
+                for m, p in enumerate(parts)
+            ]
+            result = jnp.dot(jnp.concatenate(parts, axis=1), weight, preferred_element_type=f32).astype(bf16)
+            kcat[d, pl.ds(side * half, half), :NOPE] = result[:, :NOPE]
+            vals[pl.ds(d * tokens + side * half, half), :] = result[:, NOPE:]
+
+    def score(d):
+        if d > 0:
+            rope_far[d].wait_recv()
+        packed = ropeb[d].astype(f32)
+        kcat[d, pl.ds(0, half), NOPE:] = packed.astype(bf16)
+        kcat[d, pl.ds(half, half), NOPE:] = pltpu.roll(packed, 64, 1).astype(bf16)
+        scores[:, d * tokens : (d + 1) * tokens] = lax.dot_general(
+            qcat[...], kcat[d], (((1,), (1,)), ((), ())), preferred_element_type=f32
+        )
+
+    conv_mixed = conv()
+    previous = None
+    for d in order:
+        count = pass_lat(d, count)
+        if previous is not None:
+            for m in range(chips):
+                lat_pass[previous, m].wait_recv()
+            expand(previous)
+            score(previous)
+        previous = d
+    for m in range(chips):
+        lat_pass[previous, m].wait_recv()
+    expand(previous)
+    score(previous)
+
+    s = scores[...]
+    row_max = jnp.max(s, axis=1, keepdims=True)
+    e = jnp.exp(s - row_max)
+    row_sum = jnp.sum(e, axis=1, keepdims=True)
+    summed = jnp.dot(e.astype(bf16), vals[...], preferred_element_type=f32)
+    attended = (summed / row_sum).astype(bf16)
+    both = jnp.concatenate([attended, conv_mixed], axis=1)
+
+    slice_rows = tokens // (chips * CORES)
+    width = wo.shape[1] // OUT_CHUNKS
+    pairs, crosses = {}, {}
+    for j in range(OUT_CHUNKS):
+        cols = pl.ds(j * width, width)
+        pbuf[:, cols] = jnp.dot(both, wo[:, cols], preferred_element_type=f32).astype(bf16)
+        for m in far_first + [0]:
+            rows = pl.ds(pl.multiple_of((chip_of[m] * CORES + 1 - core) * slice_rows, slice_rows), slice_rows)
+            pairs[j, m] = remote(
+                pbuf.at[rows, cols], pair_in.at[m, :, cols], pair_send.at[j, m], pair_recv.at[j, m], partner
+            )
+            pairs[j, m].start()
+            pending.append(pairs[j, m])
+    lse = row_max + jnp.log(row_sum)
+    lse_ref[...] = jnp.transpose(jnp.broadcast_to(lse, (tokens, 128)))[:1]
+
+    def mine(m, cols):
+        rows = pl.ds(pl.multiple_of((chip_of[m] * CORES + core) * slice_rows, slice_rows), slice_rows)
+        return pbuf[rows, cols].astype(f32) + pair_in[m, :, cols].astype(f32)
+
+    for j in range(OUT_CHUNKS):
+        cols = pl.ds(j * width, width)
+        for m in far_first:
+            pairs[j, m].wait_recv()
+            pair_sum[m, :, cols] = mine(m, cols).astype(bf16)
+            crosses[j, m] = remote(
+                pair_sum.at[m, :, cols], chip_in.at[m, :, cols], chip_send.at[j, m], chip_recv.at[j, m], mate[m]
+            )
+            crosses[j, m].start()
+            pending.append(crosses[j, m])
+    for j in range(OUT_CHUNKS):
+        cols = pl.ds(j * width, width)
+        pairs[j, 0].wait_recv()
+        total = mine(0, cols)
+        for m in near_first:
+            crosses[j, m].wait_recv()
+            total = total + chip_in[m, :, cols].astype(f32)
+        out_ref[:, cols] = total.astype(bf16)
+    for copy in pending:
+        copy.wait_send()
+
+
+def fused(
+    mesh,
+    activations,
+    norm_gain,
+    query_weight,
+    latent_weight,
+    rope_key_weight,
+    latent_gain,
+    expand_weight,
+    gate_weight,
+    pre_weight,
+    value_weight,
+    conv_kernel,
+    output_attend,
+    output_conv,
+):
+    splits, chips = mesh.shape["sp"], mesh.shape["tp"] // CORES
+    tokens, local = activations.shape
+    width = output_attend.shape[1]
+    bf16, f32 = jnp.bfloat16, jnp.float32
+    slice_rows = tokens // (chips * CORES)
+    table = jnp.asarray(rope_table(splits * tokens))
+    vmem, hbm = pl.BlockSpec(memory_space=pltpu.VMEM), pl.BlockSpec(memory_space=pltpu.HBM)
+    dma = pltpu.SemaphoreType.DMA
+    whole = [query_weight, latent_weight, rope_key_weight, expand_weight, gate_weight, pre_weight, value_weight]
+    return pl.pallas_call(
+        functools.partial(mixer_kernel, splits, chips),
+        out_shape=(
+            jax.ShapeDtypeStruct((slice_rows, width), bf16),
+            jax.ShapeDtypeStruct((1, tokens), f32),
+        ),
+        in_specs=[hbm, vmem, hbm, hbm, hbm, vmem, hbm, hbm, hbm, hbm, vmem, hbm, hbm, hbm],
+        out_specs=(vmem, vmem),
+        scratch_shapes=[pltpu.VMEM((chips, CORES, tokens, local), bf16)]
+        + [pltpu.VMEM(w.shape, bf16) for w in whole]
+        + [
+            pltpu.VMEM((output_attend.shape[0] + output_conv.shape[0], width), bf16),
+            pltpu.VMEM((tokens, 2 * ROPE), f32),
+            pltpu.VMEM((tokens, 128), f32),
+            pltpu.VMEM((tokens, 3 * 128), f32),
+            pltpu.VMEM((tokens, NOPE + ROPE), f32),
+            pltpu.VMEM((splits, chips, CORES, tokens // 2, 128), bf16),
+            pltpu.VMEM((splits, tokens // 2, 128), bf16),
+            pltpu.VMEM((2, 16, 128), bf16),
+            pltpu.VMEM((2, 16, 128), bf16),
+            pltpu.VMEM((tokens, 256), bf16),
+            pltpu.VMEM((splits, tokens, 256), bf16),
+            pltpu.VMEM((splits * tokens, VDIM), bf16),
+            pltpu.VMEM((tokens, splits * tokens), f32),
+            pltpu.VMEM((tokens + 16, 128), f32),
+            pltpu.VMEM((tokens, width), bf16),
+            pltpu.VMEM((chips, slice_rows, width), bf16),
+            pltpu.VMEM((chips, slice_rows, width), bf16),
+            pltpu.VMEM((chips, slice_rows, width), bf16),
+            dma((11,)),
+            dma((2 * chips,)),
+            dma((chips, 2)),
+            dma((splits * (2 * chips + 1),)),
+            dma((splits, chips, 2)),
+            dma((splits,)),
+            dma((splits,)),
+            dma((2,)),
+            dma((2,)),
+            dma((OUT_CHUNKS, chips)),
+            dma((OUT_CHUNKS, chips)),
+            dma((OUT_CHUNKS, chips)),
+            dma((OUT_CHUNKS, chips)),
+        ],
+        compiler_params=pltpu.CompilerParams(
+            collective_id=0, has_side_effects=True, vmem_limit_bytes=60 * 2**20
+        ),
+    )(
+        activations,
+        norm_gain[None],
+        query_weight,
+        latent_weight,
+        rope_key_weight,
+        latent_gain[None],
+        expand_weight,
+        gate_weight,
+        pre_weight,
+        value_weight,
+        conv_kernel,
+        output_attend,
+        output_conv,
+        table,
+    )
+
+
 def solution(mesh):
     return jax.shard_map(
-        body,
+        functools.partial(fused, mesh) if fits(mesh) else body,
         mesh=mesh,
         in_specs=(
             P("sp", "tp"),

time: 136 us -> 47.5 us (0.35)
  blocking collectives: 53.9 us -> 0 us
  waiting for transfers between devices: 40.2 us -> 0 us
  Pallas kernels: 0 us -> 39.2 us
  between operations: 14.3 us -> 0.66 us
  matrix products: 9.9 us -> 0 us
  starting transfers between devices: 5.04 us -> 0 us
  other arithmetic: 2.83 us -> 0 us
  local copies, waits for them, and re-layouts: 9.39 us -> 7.42 us
    pallas_call x0 -> x1, Pallas kernels: none -> 39.2 us  [fused(): pl.pallas_call(functools.partial(mixer_kernel, splits, chips), out_shape=...]
    all_gather x3 -> x0, blocking collectives: 38.8 us -> none  [the longest x1 16.1 us: body(): key_piece = lax.all_gather(expanded, 'sp', axis=0, tiled=True)]
    reduce_scatter x1 -> x0, waiting for transfers between devices: 34.8 us -> none  [body(): lax.psum_scatter((jnp.dot(attended, output_attend, preferred_element_type...]
    psum x1 -> x0, blocking collectives: 15.2 us -> none  [body(): lax.psum(jnp.sum(inputs_f32 * inputs_f32, axis=1, keepdims=True), 'tp')]
    dot_general x6 -> x0, matrix products: 9.9 us -> none  [the longest x1 3.22 us: body(): jnp.dot(conv_mixed, output_conv, preferred_element_type=jnp.float32)]
    ppermute x2 -> x0, starting transfers between devices: 4.97 us -> none  [the longest x1 3.67 us: with_halo(): before = lax.ppermute(last, axis, up)]
    all_gather x1 -> x0, waiting for transfers between devices: 2.68 us -> none  [body(): lax.all_gather(activations, 'tp', axis=1, tiled=True).astype(jnp.float32)]
    ppermute x2 -> x0, waiting for transfers between devices: 2.06 us -> none  [the longest x1 2.06 us: with_halo(): after = lax.ppermute(leading, axis, down)]
  transfers between devices with their start and end apart: 4 -> 0, of which waited for: 3 -> 0; matrix products, arithmetic and copies ran while one was open for 10% -> 0% of each run, Pallas kernels for 0% -> 0%
where the time goes in v1:
time: 47.5 us; the launch traced here: 47.3 us
  Pallas kernels  39.2 us (83%)
  local copies, waits for them, and re-layouts  7.42 us (16%)
  between operations  0.66 us (1%)
    pallas_call x1, Pallas kernels, fused(): pl.pallas_call(functools.partial(mixer_kernel, splits, chips), out_shape=...  39.2 us
    unnamed x9, local copies, waits for them, and re-layouts  7.42 us

profile of v1, /device:TPU:0, one launch (start us, length us, event | category | flops | bytes accessed | tf_op | source)
XLA Modules:
  0.0 47.3 jit_solution(10795348689572627456)
XLA Ops:
  0.6 0.0 copy-start
  0.6 2.0 %copy.17.wl_h = bf16[2048,64]{1,0:T(8,128)(2,1)} copy(bf16[2048,64]{0,1:T(8,128)(2,1)} %param.17) | data formatting | bytes 524288 | tf_op args[3]
  2.7 2.0 %copy.18.wr_h = bf16[2048,64]{1,0:T(8,128)(2,1)} copy(bf16[2048,64]{0,1:T(8,128)(2,1)} %param.18) | data formatting | bytes 524288 | tf_op args[4]
  4.6 0.0 copy-done
  4.6 1.3 %copy.16.wq_h = bf16[2048,192]{1,0:T(8,128)(2,1)} copy(bf16[2048,192]{0,1:T(8,128)(2,1)S(1)} %copy-done) | data formatting | bytes 1572864 | tf_op args[2]
  5.9 39.2 %shard_map.149 = (bf16[32,2048]{1,0:T(8,128)(2,1)}, f32[1,256]{1,0:T(1,128)}) custom-call(bf16[256,256]{1,0:T(8,128)(2,1)} %act.1, f32[1,2048]{1,0:T(1,128)} %bitcast.2, bf16[2048,192]{1,0:T(8,128)(2,1)} %copy.16.wq_h, bf16[2048,64]{1,0:T(8,128)(2,1)} %copy.17.wl_h, bf16[2048,64]{1,0:T(8,128)(2,1)} %copy.18.wr_h, f32[1,512]{1,0:T(1,128)} %bitcast.3, ...), custom_call_target="tpu_custom_call" | custom-call | tf_op jit(solution)/shard_map/pallas_call | solution.py:598
  45.1 0.0 copy-start.1
  45.1 1.6 %copy.21 = bf16[32,2048]{1,0:T(8,128)(2,1)} copy(bf16[32,2048]{1,0:T(8,128)(2,1)} %get-tuple-element.4) | data formatting | bytes 262144
  46.7 0.0 copy-done.1
  46.7 0.6 %copy.22 = f32[1,256]{1,0:T(1,128)} copy(f32[1,256]{1,0:T(1,128)S(1)} %copy-done.1) | data formatting | bytes 2048
Async XLA Ops:
  0.6 4.0 %copy-start = (bf16[2048,192]{0,1:T(8,128)(2,1)S(1)}, bf16[2048,192]{0,1:T(8,128)(2,1)}, u32[]{:S(2)}) copy-start(bf16[2048,192]{0,1:T(8,128)(2,1)} %param.16) | copy-start | bytes 2359300
  45.1 1.6 %copy-start.1 = (f32[1,256]{1,0:T(1,128)S(1)}, f32[1,256]{1,0:T(1,128)}, u32[]{:S(2)}) copy-start(f32[1,256]{1,0:T(1,128)} %get-tuple-element.5) | copy-start | bytes 3076

commit v2 on v1

--- a/solution.py
+++ b/solution.py
@@ -179,6 +179,7 @@
 
 
 CORES = 2
+VMEM_LIMIT = 60 * 2**20
 MAX_SPLITS = 8
 OUT_CHUNKS = 4
 MESH = pl.DeviceIdType.MESH
@@ -186,7 +187,7 @@
 
 def fits(mesh):
     chips = mesh.shape["tp"] // CORES
-    return mesh.shape["sp"] <= MAX_SPLITS and chips & (chips - 1) == 0
+    return mesh.shape["sp"] <= MAX_SPLITS and chips == 4
 
 
 def flip(index, mask, count):
@@ -237,8 +238,7 @@
     lse_ref,
     actb,
     wq,
-    wl,
-    wr,
+    wlr,
     we,
     wg,
     wp,
@@ -294,7 +294,7 @@
         )
 
     loads = [
-        (act, actb.at[0, core]), (wl_h, wl), (wr_h, wr), (wq_h, wq), (wg_h, wg), (wp_h, wp), (wv_h, wv),
+        (act, actb.at[0, core]), (wl_h, wlr.at[pl.ds(0, wl_h.shape[0])]), (wr_h, wlr.at[pl.ds(wl_h.shape[0], wr_h.shape[0])]), (wq_h, wq), (wg_h, wg), (wp_h, wp), (wv_h, wv),
         (tab_h.at[pl.ds(sp * tokens, tokens)], tab), (we_h, we),
         (oa_h, wo.at[pl.ds(0, oa_h.shape[0])]), (oc_h, wo.at[pl.ds(oa_h.shape[0], oc_h.shape[0])]),
     ]
@@ -312,20 +312,20 @@
     loads[0].wait()
     own = actb.at[0, core]
 
-    def send_act(m):
-        copy = remote(own, actb.at[m, core], act_send.at[m], act_recv.at[m, 0], mate[m])
+    def act_copy(m, slot, side, kind, device, index):
+        piece = pl.ds(side * half, half)
+        copy = remote(
+            actb.at[m, core, piece], actb.at[slot, core, piece], act_send.at[index], act_recv.at[slot, side, kind], device
+        )
         copy.start()
         pending.append(copy)
         return copy
 
-    def pass_act(m):
-        copy = remote(actb.at[m, core], actb.at[m, core], act_send.at[chips + m], act_recv.at[m, 1], partner)
-        copy.start()
-        pending.append(copy)
-        return copy
-
-    direct = {m: send_act(m) for m in far_first}
-    passed = {0: pass_act(0)}
+    direct, passed = {}, {}
+    for index, (m, side) in enumerate([(1, 0), (2, 1), (1, 1), (2, 0)]):
+        direct[m, side] = act_copy(0, m, side, 0, mate[m], index)
+    for side in range(2):
+        passed[0, side] = act_copy(0, 0, side, 1, partner, 4 + side)
     for load in loads[1:8]:
         load.wait()
 
@@ -349,11 +349,13 @@
         else:
             ref[...] += value
 
+    def across(left, right):
+        return lax.dot_general(left, right, (((1,), (1,)), ((), ())), preferred_element_type=f32)
+
     def latent_dot(m):
         for k in range(CORES):
             rows = rows_of(m, k)
-            weight = jnp.concatenate([wl[rows, :], wr[rows, :]], axis=1)
-            put(acc_l, jnp.dot(scaled[m, k], weight, preferred_element_type=f32), m == 0 and k == 0)
+            put(acc_l, across(scaled[m, k], wlr[:, rows]), m == 0 and k == 0)
 
     def other_dots(m):
         for k in range(CORES):
@@ -361,24 +363,33 @@
             first = m == 0 and k == 0
             weight = jnp.concatenate([wg[rows, :], wp[rows, :], wv[rows, :]], axis=1)
             put(acc_g, jnp.dot(scaled[m, k], weight, preferred_element_type=f32), first)
-            put(acc_q, jnp.dot(scaled[m, k], wq[rows, :], preferred_element_type=f32), first)
-
-    passed[0].wait_recv()
-    squares = scale(0, squares)
-    latent_dot(0)
-    other_dots(0)
-    for m in near_first:
-        direct[m].wait_recv()
-        passed[m] = pass_act(m)
-        if m > 1:
-            passed[m - 1].wait_recv()
-            squares = scale(m - 1, squares)
-            latent_dot(m - 1)
-            other_dots(m - 1)
+            put(acc_q, across(scaled[m, k], wq[:, rows]), first)
+
+    def arrived(m):
+        for side in range(2):
+            passed[m, side].wait_recv()
+
+    def take(m, squares, others=True):
+        arrived(m)
+        squares = scale(m, squares)
+        latent_dot(m)
+        if others:
+            other_dots(m)
+        return squares
+
+    squares = take(0, squares)
+    for index, (m, side) in enumerate([(1, 0), (2, 1), (1, 1), (2, 0)]):
+        direct[m, side].wait_recv()
+        if index < 2:
+            direct[3, side] = act_copy(m, 3, side, 0, mate[3 - m], 6 + index)
+        passed[m, side] = act_copy(m, m, side, 1, partner, 8 + index)
+    squares = take(1, squares)
+    for side in range(2):
+        direct[3, side].wait_recv()
+        passed[3, side] = act_copy(3, 3, side, 1, partner, 12 + side)
+    squares = take(2, squares)
     last = chips - 1
-    passed[last].wait_recv()
-    squares = scale(last, squares)
-    latent_dot(last)
+    squares = take(last, squares, False)
     inv_rms = lax.rsqrt(jnp.sum(squares, axis=1, keepdims=True) / (local * chips * CORES) + EPSILON)
 
     lane = lax.broadcasted_iota(jnp.int32, (half, 128), 1)
@@ -534,7 +545,8 @@
     for j in range(OUT_CHUNKS):
         cols = pl.ds(j * width, width)
         pbuf[:, cols] = jnp.dot(both, wo[:, cols], preferred_element_type=f32).astype(bf16)
-        for m in far_first + [0]:
+        first, second = (1, 2) if j % 2 == 0 else (2, 1)
+        for m in (3, first, second, 0):
             rows = pl.ds(pl.multiple_of((chip_of[m] * CORES + 1 - core) * slice_rows, slice_rows), slice_rows)
             pairs[j, m] = remote(
                 pbuf.at[rows, cols], pair_in.at[m, :, cols], pair_send.at[j, m], pair_recv.at[j, m], partner
@@ -548,24 +560,33 @@
         rows = pl.ds(pl.multiple_of((chip_of[m] * CORES + core) * slice_rows, slice_rows), slice_rows)
         return pbuf[rows, cols].astype(f32) + pair_in[m, :, cols].astype(f32)
 
-    for j in range(OUT_CHUNKS):
-        cols = pl.ds(j * width, width)
-        for m in far_first:
-            pairs[j, m].wait_recv()
-            pair_sum[m, :, cols] = mine(m, cols).astype(bf16)
-            crosses[j, m] = remote(
-                pair_sum.at[m, :, cols], chip_in.at[m, :, cols], chip_send.at[j, m], chip_recv.at[j, m], mate[m]
-            )
-            crosses[j, m].start()
-            pending.append(crosses[j, m])
-    for j in range(OUT_CHUNKS):
-        cols = pl.ds(j * width, width)
+    def cross(j, source, target, kind, device):
+        copy = remote(source, target, chip_send.at[j, kind], chip_recv.at[j, kind], device)
+        copy.start()
+        pending.append(copy)
+        crosses[j, kind] = copy
+
+    plans = [
+        (j, pl.ds(j * width, width)) + ((1, 2) if j % 2 == 0 else (2, 1)) for j in range(OUT_CHUNKS)
+    ]
+    for j, cols, first, second in plans:
+        pairs[j, 3].wait_recv()
+        pair_sum[0, :, cols] = mine(3, cols).astype(bf16)
+        cross(j, pair_sum.at[0, :, cols], chip_in.at[0, :, cols], 0, mate[first])
+        pairs[j, first].wait_recv()
+        pair_sum[1, :, cols] = mine(first, cols).astype(bf16)
+        cross(j, pair_sum.at[1, :, cols], chip_in.at[1, :, cols], 1, mate[first])
+    for j, cols, first, second in plans:
+        pairs[j, second].wait_recv()
+        crosses[j, 0].wait_recv()
+        pair_sum[2, :, cols] = (mine(second, cols) + chip_in[0, :, cols].astype(f32)).astype(bf16)
+        cross(j, pair_sum.at[2, :, cols], chip_in.at[2, :, cols], 2, mate[second])
+    for j, cols, first, second in plans:
         pairs[j, 0].wait_recv()
-        total = mine(0, cols)
-        for m in near_first:
-            crosses[j, m].wait_recv()
-            total = total + chip_in[m, :, cols].astype(f32)
-        out_ref[:, cols] = total.astype(bf16)
+        crosses[j, 1].wait_recv()
+        total = mine(0, cols) + chip_in[1, :, cols].astype(f32)
+        crosses[j, 2].wait_recv()
+        out_ref[:, cols] = (total + chip_in[2, :, cols].astype(f32)).astype(bf16)
     for copy in pending:
         copy.wait_send()
 
@@ -594,7 +615,8 @@
     table = jnp.asarray(rope_table(splits * tokens))
     vmem, hbm = pl.BlockSpec(memory_space=pltpu.VMEM), pl.BlockSpec(memory_space=pltpu.HBM)
     dma = pltpu.SemaphoreType.DMA
-    whole = [query_weight, latent_weight, rope_key_weight, expand_weight, gate_weight, pre_weight, value_weight]
+    whole = [query_weight.shape[::-1], (latent_weight.shape[1] + rope_key_weight.shape[1], latent_weight.shape[0])]
+    whole += [expand_weight.shape, gate_weight.shape, pre_weight.shape, value_weight.shape]
     return pl.pallas_call(
         functools.partial(mixer_kernel, splits, chips),
         out_shape=(
@@ -604,7 +626,7 @@
         in_specs=[hbm, vmem, hbm, hbm, hbm, vmem, hbm, hbm, hbm, hbm, vmem, hbm, hbm, hbm],
         out_specs=(vmem, vmem),
         scratch_shapes=[pltpu.VMEM((chips, CORES, tokens, local), bf16)]
-        + [pltpu.VMEM(w.shape, bf16) for w in whole]
+        + [pltpu.VMEM(shape, bf16) for shape in whole]
         + [
             pltpu.VMEM((output_attend.shape[0] + output_conv.shape[0], width), bf16),
             pltpu.VMEM((tokens, 2 * ROPE), f32),
@@ -625,8 +647,8 @@
             pltpu.VMEM((chips, slice_rows, width), bf16),
             pltpu.VMEM((chips, slice_rows, width), bf16),
             dma((11,)),
-            dma((2 * chips,)),
-            dma((chips, 2)),
+            dma((14,)),
+            dma((chips, 2, 2)),
             dma((splits * (2 * chips + 1),)),
             dma((splits, chips, 2)),
             dma((splits,)),
@@ -639,14 +661,14 @@
             dma((OUT_CHUNKS, chips)),
         ],
         compiler_params=pltpu.CompilerParams(
-            collective_id=0, has_side_effects=True, vmem_limit_bytes=60 * 2**20
+            collective_id=0, has_side_effects=True, vmem_limit_bytes=VMEM_LIMIT
         ),
     )(
         activations,
         norm_gain[None],
-        query_weight,
-        latent_weight,
-        rope_key_weight,
+        query_weight.T,
+        latent_weight.T,
+        rope_key_weight.T,
         latent_gain[None],
         expand_weight,
         gate_weight,

time: 47.5 us -> 40.6 us (0.85)
  local copies, waits for them, and re-layouts: 7.42 us -> 2.13 us
  Pallas kernels: 39.2 us -> 37.6 us
    unnamed x9 -> x4, local copies, waits for them, and re-layouts: 7.42 us -> 2.13 us
    pallas_call x1, Pallas kernels: 39.2 us -> 37.6 us  [fused(): pl.pallas_call(functools.partial(mixer_kernel, splits, chips), out_shape=...]
where the time goes in v2:
time: 40.6 us; the launch traced here: 40.4 us
  Pallas kernels  37.6 us (93%)
  local copies, waits for them, and re-layouts  2.13 us (5%)
  between operations  0.65 us (2%)
    pallas_call x1, Pallas kernels, fused(): pl.pallas_call(functools.partial(mixer_kernel, splits, chips), out_shape=...  37.6 us
    unnamed x4, local copies, waits for them, and re-layouts  2.13 us

profile of v2, /device:TPU:0, one launch (start us, length us, event | category | flops | bytes accessed | tf_op | source)
XLA Modules:
  0.0 40.4 jit_solution(15035687229502066510)
XLA Ops:
  0.6 37.6 %shard_map.149 = (bf16[32,2048]{1,0:T(8,128)(2,1)}, f32[1,256]{1,0:T(1,128)}) custom-call(bf16[256,256]{1,0:T(8,128)(2,1)} %act.1, f32[1,2048]{1,0:T(1,128)} %bitcast.8, bf16[192,2048]{1,0:T(8,128)(2,1)} %bitcast.5, bf16[64,2048]{1,0:T(8,128)(2,1)} %bitcast.6, bf16[64,2048]{1,0:T(8,128)(2,1)} %bitcast.7, f32[1,512]{1,0:T(1,128)} %bitcast.9, ...), custom_call_target="tpu_custom_call" | custom-call | tf_op jit(solution)/shard_map/pallas_call | solution.py:620
  38.2 0.0 copy-start
  38.2 1.6 %copy.18 = bf16[32,2048]{1,0:T(8,128)(2,1)} copy(bf16[32,2048]{1,0:T(8,128)(2,1)} %get-tuple-element.4) | data formatting | bytes 262144
  39.8 0.0 copy-done
  39.8 0.6 %copy.19 = f32[1,256]{1,0:T(1,128)} copy(f32[1,256]{1,0:T(1,128)S(1)} %copy-done) | data formatting | bytes 2048
Async XLA Ops:
  38.2 1.6 %copy-start = (f32[1,256]{1,0:T(1,128)S(1)}, f32[1,256]{1,0:T(1,128)}, u32[]{:S(2)}) copy-start(f32[1,256]{1,0:T(1,128)} %get-tuple-element.5) | copy-start | bytes 3076

commit v3 on v2

--- a/solution.py
+++ b/solution.py
@@ -261,7 +261,9 @@
     pair_in,
     pair_sum,
     chip_in,
+    out_buf,
     in_sem,
+    out_sem,
     act_send,
     act_recv,
     lat_send,
@@ -429,13 +431,6 @@
         jnp.where(lane < 64, cos[:half], cos[half:]),
         jnp.where(lane < 64, sin[:half], sin[half:]),
     ).astype(bf16)
-    rope_far = {}
-    for d in range(1, splits):
-        back = (splits - d) % splits
-        rope_far[back] = remote(ropeb.at[0], ropeb.at[back], rope_send.at[d], rope_recv.at[back], far[d])
-        rope_far[back].start()
-        pending.append(rope_far[back])
-
     other_dots(last)
 
     def far_wait(d):
@@ -454,15 +449,22 @@
         copy.start()
         pending.append(copy)
 
+    rope_far = {}
+    for d in range(1, splits):
+        back = (splits - d) % splits
+        rope_far[back] = remote(ropeb.at[0], ropeb.at[back], rope_send.at[d], rope_recv.at[back], far[d])
+        rope_far[back].start()
+        pending.append(rope_far[back])
+
+    factor = (NOPE + ROPE) ** (-0.5)
+    qcat[:, :NOPE] = (acc_q[:, :NOPE] * inv_rms * factor).astype(bf16)
+    tail = jnp.concatenate([acc_q[:, NOPE:], jnp.zeros((tokens, 128 - ROPE), f32)], axis=1) * inv_rms
+    qcat[:, NOPE:] = jnp.where(wide < 64, turn(tail, cos, sin) * factor, 0.0).astype(bf16)
+
     order = [0] + [d for d in (1, 3, 2) if d < splits] + list(range(4, splits))
     for d in order[1:]:
         far_wait(d)
         count = spread(d, count)
-
-    factor = (NOPE + ROPE) ** (-0.5)
-    qcat[:, :NOPE] = (acc_q[:, :NOPE] * inv_rms * factor).astype(bf16)
-    tail = jnp.concatenate([acc_q[:, NOPE:], jnp.zeros((tokens, 128 - ROPE), f32)], axis=1) * inv_rms
-    qcat[:, NOPE:] = jnp.where(wide < 64, turn(tail, cos, sin) * factor, 0.0).astype(bf16)
 
     for load in loads[8:]:
         load.wait()
@@ -516,7 +518,6 @@
             qcat[...], kcat[d], (((1,), (1,)), ((), ())), preferred_element_type=f32
         )
 
-    conv_mixed = conv()
     previous = None
     for d in order:
         count = pass_lat(d, count)
@@ -526,6 +527,7 @@
             expand(previous)
             score(previous)
         previous = d
+    conv_mixed = conv()
     for m in range(chips):
         lat_pass[previous, m].wait_recv()
     expand(previous)
@@ -566,6 +568,7 @@
         pending.append(copy)
         crosses[j, kind] = copy
 
+    stores = []
     plans = [
         (j, pl.ds(j * width, width)) + ((1, 2) if j % 2 == 0 else (2, 1)) for j in range(OUT_CHUNKS)
     ]
@@ -586,9 +589,14 @@
         crosses[j, 1].wait_recv()
         total = mine(0, cols) + chip_in[1, :, cols].astype(f32)
         crosses[j, 2].wait_recv()
-        out_ref[:, cols] = (total + chip_in[2, :, cols].astype(f32)).astype(bf16)
+        out_buf[:, cols] = (total + chip_in[2, :, cols].astype(f32)).astype(bf16)
+        copy = pltpu.make_async_copy(out_buf.at[:, cols], out_ref.at[:, cols], out_sem.at[j])
+        copy.start()
+        stores.append(copy)
     for copy in pending:
         copy.wait_send()
+    for copy in stores:
+        copy.wait()
 
 
 def fused(
@@ -624,7 +632,7 @@
             jax.ShapeDtypeStruct((1, tokens), f32),
         ),
         in_specs=[hbm, vmem, hbm, hbm, hbm, vmem, hbm, hbm, hbm, hbm, vmem, hbm, hbm, hbm],
-        out_specs=(vmem, vmem),
+        out_specs=(hbm, vmem),
         scratch_shapes=[pltpu.VMEM((chips, CORES, tokens, local), bf16)]
         + [pltpu.VMEM(shape, bf16) for shape in whole]
         + [
@@ -646,7 +654,9 @@
             pltpu.VMEM((chips, slice_rows, width), bf16),
             pltpu.VMEM((chips, slice_rows, width), bf16),
             pltpu.VMEM((chips, slice_rows, width), bf16),
+            pltpu.VMEM((slice_rows, width), bf16),
             dma((11,)),
+            dma((OUT_CHUNKS,)),
             dma((14,)),
             dma((chips, 2, 2)),
             dma((splits * (2 * chips + 1),)),

time: 40.6 us -> 41.1 us (1.012)
  Pallas kernels: 37.6 us -> 38.1 us
    pallas_call x1, Pallas kernels: 37.6 us -> 38.1 us  [fused(): pl.pallas_call(functools.partial(mixer_kernel, splits, chips), out_shape=...]
where the time goes in v3:
time: 41.1 us; the launch traced here: 40.9 us
  Pallas kernels  38.1 us (93%)
  local copies, waits for them, and re-layouts  2.13 us (5%)
  between operations  0.65 us (2%)
    pallas_call x1, Pallas kernels, fused(): pl.pallas_call(functools.partial(mixer_kernel, splits, chips), out_shape=...  38.1 us
    unnamed x4, local copies, waits for them, and re-layouts  2.13 us

profile of v3, /device:TPU:0, one launch (start us, length us, event | category | flops | bytes accessed | tf_op | source)
XLA Modules:
  0.0 40.9 jit_solution(8007660528677274503)
XLA Ops:
  0.6 38.1 %shard_map.149 = (bf16[32,2048]{1,0:T(8,128)(2,1)}, f32[1,256]{1,0:T(1,128)}) custom-call(bf16[256,256]{1,0:T(8,128)(2,1)} %act.1, f32[1,2048]{1,0:T(1,128)} %bitcast.8, bf16[192,2048]{1,0:T(8,128)(2,1)} %bitcast.5, bf16[64,2048]{1,0:T(8,128)(2,1)} %bitcast.6, bf16[64,2048]{1,0:T(8,128)(2,1)} %bitcast.7, f32[1,512]{1,0:T(1,128)} %bitcast.9, ...), custom_call_target="tpu_custom_call" | custom-call | tf_op jit(solution)/shard_map/pallas_call | solution.py:628
  38.8 0.0 copy-start
  38.8 1.6 %copy.18 = bf16[32,2048]{1,0:T(8,128)(2,1)} copy(bf16[32,2048]{1,0:T(8,128)(2,1)} %get-tuple-element.4) | data formatting | bytes 262144
  40.4 0.0 copy-done
  40.4 0.6 %copy.19 = f32[1,256]{1,0:T(1,128)} copy(f32[1,256]{1,0:T(1,128)S(1)} %copy-done) | data formatting | bytes 2048
Async XLA Ops:
  38.8 1.6 %copy-start = (f32[1,256]{1,0:T(1,128)S(1)}, f32[1,256]{1,0:T(1,128)}, u32[]{:S(2)}) copy-start(f32[1,256]{1,0:T(1,128)} %get-tuple-element.5) | copy-start | bytes 3076
